TPU v7x, 256 devices: a whole 4x4x8 slice. The times are simulated.
256 devices in a mesh: ep: 16 (over y, x), tp: 16 (over z, core).
Axes of the slice: x: 4, y: 4, z: 8, core: 2. Of those that a mesh axis runs over, the one named last changes fastest.
Arguments:
- pool_input: bfloat16 [32768, 1024], P('ep', 'tp'), may hold values from -6 to 6
- pool_gain: float32 [1024], P('tp'), may hold values from 0.1 to 1.9
- mix_weight: bfloat16 [1024, 2048], P('tp'), may hold values from -0.1875 to 0.1875
- moe_input: bfloat16 [65536, 2048], P(('ep', 'tp')), may hold values from -6 to 6
- moe_gain: float32 [2048], replicated, may hold values from 0.1 to 1.9
- expert_ids: int32 [65536, 2], P(('ep', 'tp')), may hold values from 0 to 15, as said below
- route_weight: float32 [65536, 2], P(('ep', 'tp')), may hold values from 0.2 to 1
- gate_weight: bfloat16 [16, 2048, 1024], P('ep', None, 'tp'), may hold values from -0.125 to 0.125
- up_weight: bfloat16 [16, 2048, 1024], P('ep', None, 'tp'), may hold values from -0.125 to 0.125
- down_weight: bfloat16 [16, 2048, 1024], P('ep', None, 'tp'), may hold values from -0.1875 to 0.1875
Outputs:
- mixed_out: bfloat16 [32768, 2048], P(('ep', 'tp'))
- moe_out: bfloat16 [65536, 2048], P(('ep', 'tp'))
Inputs may be any that keep to these rules, and one draw needn't show every extreme that they name: `expert_ids`: each row names 2 different experts of one group of 4 consecutive experts. In each aligned block of 256 rows (the rows of one device) no expert is named by more than 48 rows, and some expert is named by exactly 48 rows.
All inputs are finite; a program needn't handle non-finite values.
Results may differ from a plain program's by a relative error of at most 0.012.
Values may be sent and summed in bfloat16 or wider, within the bound.
A program may use at most 128 MiB of HBM per device.

v0:
```python
import jax
import jax.numpy as jnp
from jax import lax
from jax.sharding import PartitionSpec as P

GROUP_CH = 256
EXPERTS = 16
TOP = 2
CAP = 48
eps_norm = 1e-06


def from_behind(shard, axis, by):
    peers = lax.axis_size(axis)
    pairs = [(i, i + by) for i in range(peers) if 0 <= i + by < peers]
    return lax.ppermute(shard, axis, pairs)


def gather_turned(arrays, axis, dims):
    turned = [jnp.moveaxis(a, dim, 0) for a, dim in zip(arrays, dims)]
    both = jnp.concatenate([t.reshape(len(t), -1) for t in turned], axis=1)
    result, at, gathered = (lax.all_gather(both, axis, axis=0, tiled=True), 0, [])
    for t, dim in zip(turned, dims):
        section = result[:, at : at + t[0].size].reshape(-1, *t.shape[1:])
        gathered.append(jnp.moveaxis(section, 0, dim))
        at += t[0].size
    return tuple(gathered)


def in_blocks(shard, dim, peers):
    before, after = (shard.shape[:dim], shard.shape[dim + 1 :])
    return jnp.moveaxis(shard.reshape(*before, peers, -1, *after), dim, 0)


def cut_rows(length, count):
    unit = 8 if length >= 8 * count else 1
    return [length // unit * k // count * unit for k in range(1, count)]


def joined_along(tiles, dim):
    tiles = jnp.moveaxis(tiles, 0, dim)
    dims = tiles.shape
    return tiles.reshape(*dims[:dim], dims[dim] * dims[dim + 1], *dims[dim + 2 :])


def exchange_in_pieces(shard, axis, pieces, split_dim, concat_dim):
    tiles = in_blocks(shard, split_dim, lax.axis_size(axis))
    widest = max(range(1, max(2, tiles.ndim - 1)), key=lambda d: tiles.shape[d])
    gathered = []
    for section in jnp.split(tiles, cut_rows(tiles.shape[widest], pieces), axis=widest):
        if section.size:
            gathered.append(lax.all_to_all(section, axis, split_axis=0, concat_axis=0, tiled=True))
    return joined_along(jnp.concatenate(gathered, axis=widest), concat_dim)


def window_sums(extended, row_count):
    level_sum = extended
    stride = 1
    outputs = []
    for doubling in range(4):
        level_sum = level_sum[stride:] + level_sum[:-stride]
        stride = stride * 2
        outputs.append(level_sum[level_sum.shape[0] - row_count :])
    return outputs


def pool_mixer(pool_input, pool_gain):
    row_count, channels = pool_input.shape
    carried = from_behind(pool_input[row_count - 15 :], "ep", 1)
    extended = jnp.concatenate([carried, pool_input], axis=0).astype(jnp.float32)
    window_list = window_sums(extended, row_count)
    channel_ids = lax.axis_index("tp") * channels + lax.iota(jnp.int32, channels)
    group_ids = channel_ids // GROUP_CH
    position = lax.axis_index("ep") * row_count + lax.iota(jnp.int32, row_count)
    summed = jnp.zeros((row_count, channels), jnp.float32)
    widths = jnp.zeros((channels,), jnp.int32)
    for index_group in range(4):
        inside = group_ids == index_group
        summed = jnp.where(inside[None, :], window_list[index_group], summed)
        widths = jnp.where(inside, 2 ** (index_group + 1), widths)
    counted = jnp.minimum(position[:, None] + 1, widths[None, :]).astype(jnp.float32)
    values = extended[15:]
    return ((summed / counted - values) * pool_gain).astype(jnp.bfloat16)


def route_slots(expert_ids):
    flat_ids = expert_ids.reshape(-1)
    marked = (flat_ids[:, None] == lax.iota(jnp.int32, EXPERTS)[None, :]).astype(jnp.int32)
    before_count = jnp.cumsum(marked, axis=0) - marked
    ranked = jnp.sum(before_count * marked, axis=1)
    return (flat_ids * CAP + ranked).reshape(expert_ids.shape)


def body(
    pool_input,
    pool_gain,
    mix_weight,
    moe_input,
    moe_gain,
    expert_ids,
    route_weight,
    gate_weight,
    up_weight,
    down_weight,
):
    pooled = pool_mixer(pool_input, pool_gain)
    mixed_sum = lax.psum_scatter(
        jnp.dot(pooled, mix_weight, preferred_element_type=jnp.float32).astype(jnp.bfloat16),
        "tp",
        scatter_dimension=0,
        tiled=True,
    )
    inputs = moe_input.astype(jnp.float32)
    scale_rows = lax.rsqrt(jnp.mean(inputs * inputs, axis=-1, keepdims=True) + eps_norm)
    normed = (inputs * scale_rows * moe_gain).astype(jnp.bfloat16)
    slots = route_slots(expert_ids)
    slot_index = lax.iota(jnp.int32, EXPERTS * CAP)
    placing = (
        (slot_index[:, None] == slots[None, :, 0]) | (slot_index[:, None] == slots[None, :, 1])
    ).astype(jnp.bfloat16)
    outgoing = jnp.dot(placing, normed, preferred_element_type=jnp.float32).astype(jnp.bfloat16)
    outgoing = outgoing.reshape(EXPERTS, CAP, normed.shape[1])
    arrived = lax.all_to_all(outgoing, "ep", split_axis=0, concat_axis=1, tiled=True)
    gate_piece, up_piece, down_piece = gather_turned(
        (gate_weight, up_weight, down_weight), "tp", (2, 2, 2)
    )
    gate_part = jnp.einsum("erd,edf->erf", arrived, gate_piece, preferred_element_type=jnp.float32)
    upward = jnp.einsum("erd,edf->erf", arrived, up_piece, preferred_element_type=jnp.float32)
    hidden = (jax.nn.silu(gate_part) * upward).astype(jnp.bfloat16)
    expert_sum = jnp.einsum("erf,edf->erd", hidden, down_piece, preferred_element_type=jnp.float32)
    expert_rows = expert_sum.astype(jnp.bfloat16)
    returned = exchange_in_pieces(expert_rows, "ep", 2, 1, 0)
    returned_rows = returned.reshape(EXPERTS * CAP, returned.shape[2])
    combined = jnp.zeros((normed.shape[0], normed.shape[1]), jnp.float32)
    for route_index in range(TOP):
        picking = (slots[:, route_index][:, None] == slot_index[None, :]).astype(jnp.bfloat16)
        chosen_rows = jnp.dot(picking, returned_rows, preferred_element_type=jnp.float32)
        combined = combined + route_weight[:, route_index : route_index + 1] * chosen_rows
    moe_out = combined.astype(jnp.bfloat16)
    return (mixed_sum, moe_out)


def solution(mesh):
    return jax.shard_map(
        body,
        mesh=mesh,
        in_specs=(
            P("ep", "tp"),
            P("tp"),
            P("tp", None),
            P(("ep", "tp"), None),
            P(),
            P(("ep", "tp"), None),
            P(("ep", "tp"), None),
            P("ep", None, "tp"),
            P("ep", None, "tp"),
            P("ep", None, "tp"),
        ),
        out_specs=(P(("ep", "tp"), None), P(("ep", "tp"), None)),
        check_vma=False,
    )
```

profile of v0, /device:TPU:24, one launch (start us, length us, event | category | flops | bytes accessed | tf_op | source)
XLA Modules:
  0.0 169.4 jit_solution(2128738845076339087)
XLA Ops:
  7.2 0.0 copy-start
  7.2 0.0 all-gather.2.cloned.1.call-start
  7.2 2.1 %pad_maximum_fusion.1 = bf16[64,6144]{1,0:T(8,128)(2,1)} fusion(bf16[64,2048]{1,0:T(8,128)(2,1)} %bitcast.76, bf16[64,2048]{1,0:T(8,128)(2,1)} %bitcast.77, bf16[64,2048]{1,0:T(8,128)(2,1)} %bitcast.78), kind=kLoop, calls=%fused_computation.22 | loop fusion | flops 2359296 | bytes 1572864 | tf_op jit(solution)/shard_map/concatenate | solution.py:21
  9.3 0.0 all-gather.2.cloned.1.call-update
  9.3 0.0 copy-start.4
  9.3 0.0 reduce-scatter.2.cloned.1.call-start
  9.4 0.8 slice.66
  10.2 3.4 %collective-permute-start = (bf16[15,64]{0,1:T(8,128)(2,1)S(1)}, bf16[15,64]{0,1:T(8,128)(2,1)S(1)}, u32[]{:S(2)}, u32[]{:S(2)}) collective-permute-start(bf16[15,64]{0,1:T(8,128)(2,1)S(1)} %slice.66), channel_id=1, source_target_pairs={{0,16},{16,32},{32,48},{48,64},{64,80},{80,96},{96,112},{112,128},... | collective-permute-start | bytes 5768 | tf_op jit(solution)/shard_map/ppermute | solution.py:16
  13.7 4.3 %collective-permute-done = bf16[15,64]{0,1:T(8,128)(2,1)S(1)} collective-permute-done((bf16[15,64]{0,1:T(8,128)(2,1)S(1)}, bf16[15,64]{0,1:T(8,128)(2,1)S(1)}, u32[]{:S(2)}, u32[]{:S(2)}) %collective-permute-start) | collective-permute-done | bytes 1952 | tf_op jit(solution)/shard_map/ppermute | solution.py:16
  17.9 1.1 maximum_convert_fusion
  19.0 0.2 slice_add_fusion.2
  19.2 0.2 slice_add_fusion.1
  19.5 0.2 slice_add_fusion
  19.7 0.0 copy-done
  19.7 0.0 copy-done.4
  19.7 6.5 %convolution_convert_fusion = bf16[2048,2048]{1,0:T(8,128)(2,1)} fusion(bf16[64,2048]{1,0:T(8,128)(2,1)S(1)} %copy-done, f32[2063,64]{0,1:T(8,128)S(1)} %maximum_convert_fusion, f32[2062,64]{0,1:T(8,128)S(1)} %slice_add_fusion.2, f32[2060,64]{0,1:T(8,128)S(1)} %slice_add_fusion.1, f32[2056,64]{0,1:T(8,128)S(1)} %slice_add_fusion, f32[64]{0:T(128)S(1)} %copy-done.4, ...), kind=kOutput, calls=%fused_computation | convolution fusion | flops 542507008 | bytes 11283456 | tf_op jit(solution)/shard_map/dot_general | solution.py:108
  26.2 0.0 copy-start.3
  26.2 0.0 copy-start.1
  26.2 0.0 copy-start.2
  26.2 0.0 reduce-scatter.2.cloned.1.call-update
  26.2 0.7 copy-done.3
  26.9 0.1 copy.29
  27.0 0.1 eq.138
  27.1 0.1 eq.134
  27.3 1.2 reduce-window.6
  28.5 0.2 slice_reduce_fusion
  28.7 0.1 fusion.35
  28.8 0.1 reduce_sum.21
  29.0 0.1 copy.32
  29.0 0.0 copy-done.1
  29.0 0.3 fusion.6
  29.4 0.0 copy-done.2
  29.4 1.1 convolution_convert_fusion.1
  30.5 41.2 %all_to_all.19 = bf16[16,48,2048]{2,1,0:T(8,128)(2,1)S(1)} all-to-all(bf16[16,48,2048]{2,1,0:T(8,128)(2,1)S(1)} %bitcast.72), channel_id=1, replica_groups=mesh['ep'=16,'tp'=16] {'ep'}, dimensions={0} | all-to-all | bytes 6291456 | tf_op jit(solution)/shard_map/all_to_all | solution.py:123
  71.7 17.0 %all-gather.2.cloned.1.call-done = bf16[1024,6144]{1,0:T(8,128)(2,1)} async-done(((bf16[64,6144]{1,0:T(8,128)(2,1)}), bf16[1024,6144]{1,0:T(8,128)(2,1)}) %all-gather.2.cloned.1.call-update) | async-done | bytes 12582928 | tf_op jit(solution)/shard_map/all_gather | solution.py:22
  88.7 0.0 copy-start.6
  88.7 5.4 %fusion.1 = f32[768,1024]{1,0:T(8,128)S(1)} fusion(bf16[768,2048]{1,0:T(8,128)(2,1)S(1)} %bitcast.73, bf16[1024,6144]{1,0:T(8,128)(2,1)} %all-gather.2.cloned.1.call-done), kind=kOutput, calls=%fused_computation.4 | convolution fusion | flops 3221225472 | bytes 10485760 | tf_op jit(solution)/shard_map/erd,edf->erf/dot_general | solution.py:128
  94.1 0.4 copy-done.6
  94.6 3.9 %multiply_convert_fusion = bf16[768,1024]{1,0:T(8,128)(2,1)S(1)} fusion(f32[768,1024]{1,0:T(8,128)S(1)} %fusion.1, bf16[768,2048]{1,0:T(8,128)(2,1)S(1)} %bitcast.74, bf16[1024,6144]{1,0:T(8,128)(2,1)S(1)} %copy-done.6), kind=kOutput, calls=%fused_computation.10 | convolution fusion | flops 3225944064 | bytes 12058624 | tf_op jit(solution)/shard_map/erd,edf->erf/dot_general | solution.py:127
  98.4 3.6 %fusion.3 = bf16[768,2048]{1,0:T(8,128)(2,1)S(1)} fusion(bf16[768,1024]{1,0:T(8,128)(2,1)S(1)} %multiply_convert_fusion, bf16[1024,6144]{1,0:T(8,128)(2,1)S(1)} %copy-done.6), kind=kOutput, calls=%fused_computation.7 | convolution fusion | flops 3222798336 | bytes 8912896 | tf_op jit(solution)/shard_map/erf,edf->erd/dot_general | solution.py:130
  102.1 1.4 fusion.38
  103.5 0.0 copy-start.5
  103.5 28.0 %all_to_all.20 = bf16[16,1,24,2048]{3,2,1,0:T(8,128)(2,1)S(1)} all-to-all(bf16[16,1,24,2048]{3,2,1,0:T(8,128)(2,1)S(1)} %get-tuple-element.2), channel_id=1, replica_groups=mesh['ep'=16,'tp'=16] {'ep'}, dimensions={0} | all-to-all | bytes 3145728 | tf_op jit(solution)/shard_map/all_to_all | solution.py:52
  131.5 6.0 %all-to-all-start.2 = ((bf16[16,1,24,2048]{3,2,1,0:T(8,128)(2,1)}), bf16[16,1,24,2048]{3,2,1,0:T(8,128)(2,1)S(1)}, u32[]{:S(2)}, u32[]{:S(2)}) async-start(bf16[16,1,24,2048]{3,2,1,0:T(8,128)(2,1)} %get-tuple-element.3), calls=%async_computation.3 | async-start | bytes 3145728 | tf_op jit(solution)/shard_map/all_to_all | solution.py:52
  137.4 0.0 copy-done.5
  137.5 21.1 %all-to-all-done.2 = bf16[16,1,24,2048]{3,2,1,0:T(8,128)(2,1)S(1)} async-done(((bf16[16,1,24,2048]{3,2,1,0:T(8,128)(2,1)}), bf16[16,1,24,2048]{3,2,1,0:T(8,128)(2,1)S(1)}, u32[]{:S(2)}, u32[]{:S(2)}) %all-to-all-start.2) | async-done | bytes 1572896 | tf_op jit(solution)/shard_map/all_to_all | solution.py:52
  158.5 0.4 pad_maximum_fusion
  158.9 1.1 convolution_multiply_fusion.1
  160.0 2.1 %fusion.5 = bf16[256,2048]{1,0:T(8,128)(2,1)} fusion(f32[256,2048]{1,0:T(8,128)S(1)} %convolution_multiply_fusion.1, bf16[768,2048]{1,0:T(8,128)(2,1)S(1)} %bitcast.71, f32[256]{0:T(256)S(1)} %bitcast.81, s32[256]{0:T(256)S(1)} %bitcast.80), kind=kOutput, calls=%fused_computation.16 | convolution fusion | flops 807075840 | bytes 6293504 | tf_op jit(solution)/shard_map/dot_general | solution.py:137
  162.1 0.4 reduce-scatter.2.cloned.1.call-done
  (11 shorter events, 0.1 us)
Async XLA Ops:
  7.2 12.5 %copy-start = (bf16[64,2048]{1,0:T(8,128)(2,1)S(1)}, bf16[64,2048]{1,0:T(8,128)(2,1)}, u32[]{:S(2)}) copy-start(bf16[64,2048]{1,0:T(8,128)(2,1)} %param.12) | copy-start | bytes 786436
  7.2 81.5 %all-gather.2.cloned.1.call-start = ((), (), s32[]{:S(2)}) async-start(), calls=%async_computation.5 | async-start | bytes 13369344 | tf_op jit(solution)/shard_map/all_gather | solution.py:22
  9.3 10.4 %copy-start.4 = (f32[64]{0:T(128)S(1)}, f32[64]{0:T(128)}, u32[]{:S(2)}) copy-start(f32[64]{0:T(128)} %param.11) | copy-start | bytes 772
  9.3 153.2 %reduce-scatter.2.cloned.1.call-start = ((), (), s32[]{:S(2)}) async-start(), calls=%async_computation.4 | async-start | bytes 8912896 | tf_op jit(solution)/shard_map/reduce_scatter | solution.py:107
  10.2 7.7 %collective-permute-start = (bf16[15,64]{0,1:T(8,128)(2,1)S(1)}, bf16[15,64]{0,1:T(8,128)(2,1)S(1)}, u32[]{:S(2)}, u32[]{:S(2)}) collective-permute-start(bf16[15,64]{0,1:T(8,128)(2,1)S(1)} %slice.66), channel_id=1, source_target_pairs={{0,16},{16,32},{32,48},{48,64},{64,80},{80,96},{96,112},{112,128},... | collective-permute-start | bytes 5768 | tf_op jit(solution)/shard_map/ppermute | solution.py:16
  26.2 0.7 copy-start.3
  26.2 2.9 %copy-start.1 = (bf16[256,2048]{1,0:T(8,128)(2,1)S(1)}, bf16[256,2048]{1,0:T(8,128)(2,1)}, u32[]{:S(2)}) copy-start(bf16[256,2048]{1,0:T(8,128)(2,1)} %param.13) | copy-start | bytes 3145732
  26.2 3.2 %copy-start.2 = (f32[2048]{0:T(1024)S(1)}, f32[2048]{0:T(1024)}, u32[]{:S(2)}) copy-start(f32[2048]{0:T(1024)} %param.14) | copy-start | bytes 24580
  88.7 5.8 %copy-start.6 = (bf16[1024,6144]{1,0:T(8,128)(2,1)S(1)}, bf16[1024,6144]{1,0:T(8,128)(2,1)}, u32[]{:S(2)}) copy-start(bf16[1024,6144]{1,0:T(8,128)(2,1)} %all-gather.2.cloned.1.call-done) | copy-start | bytes 37748740
  103.5 34.0 %copy-start.5 = (f32[256,2]{0,1:T(2,128)S(1)}, f32[256,2]{0,1:T(2,128)}, u32[]{:S(2)}) copy-start(f32[256,2]{0,1:T(2,128)} %param.16) | copy-start | bytes 6148
  131.5 27.0 %all-to-all-start.2 = ((bf16[16,1,24,2048]{3,2,1,0:T(8,128)(2,1)}), bf16[16,1,24,2048]{3,2,1,0:T(8,128)(2,1)S(1)}, u32[]{:S(2)}, u32[]{:S(2)}) async-start(bf16[16,1,24,2048]{3,2,1,0:T(8,128)(2,1)} %get-tuple-element.3), calls=%async_computation.3 | async-start | bytes 3145728 | tf_op jit(solution)/shard_map/all_to_all | solution.py:52
Sparse Core Ops, SparseCore 0:
  10.4 78.2 all-gather.1
  91.8 70.6 reduce-scatter.1
where the time goes:
time: 170 us; the launch traced here: 169 us
  blocking collectives  69.2 us (41%)
  waiting for transfers between devices  42.8 us (25%)
  matrix products  23.8 us (14%)
  between operations  14.3 us (8%)
  starting transfers between devices  9.42 us (6%)
  other arithmetic  5.79 us (3%)
  local copies, waits for them, and re-layouts  4.17 us (2%)
    all_to_all x1, blocking collectives, body(): lax.all_to_all(outgoing, 'ep', split_axis=0, concat_axis=1, tiled=True)  41.2 us
    all_to_all x1, blocking collectives, exchange_in_pieces(): lax.all_to_all(section, axis, split_axis=0, concat_axis=0, tiled=True)  28 us
    all_to_all x1, waiting for transfers between devices, exchange_in_pieces(): lax.all_to_all(section, axis, split_axis=0, concat_axis=0, tiled=True)  21.1 us
    all_gather x1, waiting for transfers between devices, gather_turned(): lax.all_gather(both, axis, axis=0, tiled=True)  17 us
    dot_general x1, matrix products, body(): jnp.dot(pooled, mix_weight, preferred_element_type=jnp.float32)  6.48 us
    all_to_all x1, starting transfers between devices, exchange_in_pieces(): lax.all_to_all(section, axis, split_axis=0, concat_axis=0, tiled=True)  5.95 us
    dot_general x1, matrix products, body(): jnp.einsum('erd,edf->erf', arrived, up_piece, preferred_element_type=jnp....  5.42 us
    ppermute x1, waiting for transfers between devices, from_behind(): return lax.ppermute(shard, axis, pairs)  4.26 us
  transfers between devices with their start and end apart: 4, of which 4 were waited for; matrix products, arithmetic and copies ran while one was open for 18% of the time, Pallas kernels for 0%

commit v1 on v0

--- a/solution.py
+++ b/solution.py
@@ -19,7 +19,16 @@
 def gather_turned(arrays, axis, dims):
     turned = [jnp.moveaxis(a, dim, 0) for a, dim in zip(arrays, dims)]
     both = jnp.concatenate([t.reshape(len(t), -1) for t in turned], axis=1)
-    result, at, gathered = (lax.all_gather(both, axis, axis=0, tiled=True), 0, [])
+    _drive_bench = lambda net_axis, inp: jnp.concatenate(
+        jax.lax.all_to_all(
+            jnp.stack([inp for _ in range(jax.lax.axis_size(net_axis))]),
+            net_axis,
+            split_axis=0,
+            concat_axis=0,
+        ),
+        axis=0,
+    )
+    result, at, gathered = (_drive_bench(axis, both), 0, [])
     for t, dim in zip(turned, dims):
         section = result[:, at : at + t[0].size].reshape(-1, *t.shape[1:])
         gathered.append(jnp.moveaxis(section, 0, dim))

time: 170 us -> 486 us (2.86)
  waiting for transfers between devices: 42.8 us -> 373 us
  blocking collectives: 69.2 us -> 27 us
  starting transfers between devices: 9.42 us -> 24.1 us
  matrix products: 23.8 us -> 32.7 us
  local copies, waits for them, and re-layouts: 4.17 us -> 9.12 us
    all_to_all x0 -> x2, waiting for transfers between devices: none -> 346 us  [the longest x1 299 us: gather_turned(): jax.lax.all_to_all(jnp.stack([inp for _ in range(jax.lax.axis_size(net_ax...]
    all_to_all x1 -> x0, blocking collectives: 41.2 us -> none  [body(): lax.all_to_all(outgoing, 'ep', split_axis=0, concat_axis=1, tiled=True)]
    all_gather x1 -> x0, waiting for transfers between devices: 17 us -> none  [gather_turned(): lax.all_gather(both, axis, axis=0, tiled=True)]
    all_to_all x0 -> x2, starting transfers between devices: none -> 16.1 us  [the longest x1 8.76 us: gather_turned(): jax.lax.all_to_all(jnp.stack([inp for _ in range(jax.lax.axis_size(net_ax...]
    another operation x1 -> x2, local copies, waits for them, and re-layouts: 0.01 us -> 6.04 us  [the longest x1 6.04 us: gather_turned(): jnp.stack([inp for _ in range(jax.lax.axis_size(net_axis))])]
  transfers between devices with their start and end apart: 4 -> 5, of which waited for: 4 -> 4; matrix products, arithmetic and copies ran while one was open for 18% -> 6% of each run, Pallas kernels for 0% -> 0%
where the time goes in v1:
time: 486 us; the launch traced here: 485 us
  waiting for transfers between devices  373 us (77%)
  matrix products  32.7 us (7%)
  blocking collectives  27 us (6%)
  starting transfers between devices  24.1 us (5%)
  between operations  14.2 us (3%)
  local copies, waits for them, and re-layouts  9.12 us (2%)
    all_to_all x1, waiting for transfers between devices, gather_turned(): jax.lax.all_to_all(jnp.stack([inp for _ in range(jax.lax.axis_size(net_ax...  299 us
    all_to_all x1, waiting for transfers between devices, body(): lax.all_to_all(outgoing, 'ep', split_axis=0, concat_axis=1, tiled=True)  46.3 us
    all_to_all x1, blocking collectives, exchange_in_pieces(): lax.all_to_all(section, axis, split_axis=0, concat_axis=0, tiled=True)  27 us
    all_to_all x1, waiting for transfers between devices, exchange_in_pieces(): lax.all_to_all(section, axis, split_axis=0, concat_axis=0, tiled=True)  21.8 us
  transfers between devices with their start and end apart: 5, of which 4 were waited for; matrix products, arithmetic and copies ran while one was open for 6% of the time, Pallas kernels for 0%

profile of v1, /device:TPU:24, one launch (start us, length us, event | category | flops | bytes accessed | tf_op | source)
XLA Modules:
  0.0 484.8 jit_solution(15221966588826953785)
XLA Ops:
  7.2 0.0 copy-start
  7.2 0.9 copy.29
  8.0 0.1 eq.138
  8.2 0.1 eq.134
  8.3 1.2 reduce-window.6
  9.5 0.2 slice_reduce_fusion
  9.8 0.1 fusion.35
  9.9 0.1 reduce_sum.21
  10.0 0.1 copy.32
  10.1 0.7 multiply_add_fusion
  10.8 1.5 fusion.6
  12.3 4.0 convolution_convert_fusion.1
  16.3 0.0 copy-start.2
  16.3 0.0 copy-start.3
  16.3 0.0 copy-start.4
  16.3 7.3 %all-to-all-start = ((bf16[16,48,2048]{2,1,0:T(8,128)(2,1)}), bf16[16,48,2048]{2,1,0:T(8,128)(2,1)}, u32[]{:S(2)}, u32[]{:S(2)}) async-start(bf16[16,48,2048]{2,1,0:T(8,128)(2,1)} %bitcast.4), calls=%async_computation.1 | async-start | bytes 6291456 | tf_op jit(solution)/shard_map/all_to_all | solution.py:132
  23.6 0.0 copy-done.2
  23.6 0.0 copy-done.3
  23.6 0.0 copy-done.4
  23.6 0.1 pad_maximum_fusion.1
  23.7 46.3 %all-to-all-done = bf16[16,48,2048]{2,1,0:T(8,128)(2,1)} async-done(((bf16[16,48,2048]{2,1,0:T(8,128)(2,1)}), bf16[16,48,2048]{2,1,0:T(8,128)(2,1)}, u32[]{:S(2)}, u32[]{:S(2)}) %all-to-all-start) | async-done | bytes 3145760 | tf_op jit(solution)/shard_map/all_to_all | solution.py:132
  70.0 6.0 %stack.2 = bf16[16,64,6144]{2,1,0:T(8,128)(2,1)} broadcast(bf16[64,6144]{1,0:T(8,128)(2,1)S(1)} %pad_maximum_fusion.1), dimensions={1,2} | broadcast | bytes 13369344 | tf_op jit(solution)/shard_map/stack | solution.py:24
  76.0 0.0 copy-start.1
  76.0 8.8 %all-to-all-start.1 = ((bf16[16,64,6144]{2,1,0:T(8,128)(2,1)}), bf16[16,64,6144]{2,1,0:T(8,128)(2,1)}, u32[]{:S(2)}, u32[]{:S(2)}) async-start(bf16[16,64,6144]{2,1,0:T(8,128)(2,1)} %stack.2), calls=%async_computation.2 | async-start | bytes 25165824 | tf_op jit(solution)/shard_map/all_to_all | solution.py:23
  84.8 0.0 copy-start.5
  84.8 0.0 reduce-scatter.2.cloned.1.call-start
  84.8 0.0 copy-done.1
  84.8 0.1 slice.66
  84.9 2.1 collective-permute-start
  87.1 5.6 %collective-permute-done = bf16[15,64]{0,1:T(8,128)(2,1)S(1)} collective-permute-done((bf16[15,64]{0,1:T(8,128)(2,1)S(1)}, bf16[15,64]{0,1:T(8,128)(2,1)S(1)}, u32[]{:S(2)}, u32[]{:S(2)}) %collective-permute-start) | collective-permute-done | bytes 1952 | tf_op jit(solution)/shard_map/ppermute | solution.py:16
  92.7 0.1 maximum_convert_fusion
  92.8 0.2 slice_add_fusion.2
  93.0 0.2 slice_add_fusion.1
  93.2 0.2 slice_add_fusion
  93.4 0.0 copy-done
  93.5 0.0 copy-done.5
  93.5 6.4 %convolution_convert_fusion = bf16[2048,2048]{1,0:T(8,128)(2,1)} fusion(bf16[64,2048]{1,0:T(8,128)(2,1)S(1)} %copy-done, f32[2063,64]{0,1:T(8,128)S(1)} %maximum_convert_fusion, f32[2062,64]{0,1:T(8,128)S(1)} %slice_add_fusion.2, f32[2060,64]{0,1:T(8,128)S(1)} %slice_add_fusion.1, f32[2056,64]{0,1:T(8,128)S(1)} %slice_add_fusion, f32[64]{0:T(128)S(1)} %copy-done.5, ...), kind=kOutput, calls=%fused_computation | convolution fusion | flops 542507008 | bytes 11283456 | tf_op jit(solution)/shard_map/dot_general | solution.py:117
  99.8 0.0 reduce-scatter.2.cloned.1.call-update
  99.8 299.4 %all-to-all-done.1 = bf16[16,64,6144]{2,1,0:T(8,128)(2,1)} async-done(((bf16[16,64,6144]{2,1,0:T(8,128)(2,1)}), bf16[16,64,6144]{2,1,0:T(8,128)(2,1)}, u32[]{:S(2)}, u32[]{:S(2)}) %all-to-all-start.1) | async-done | bytes 12582944 | tf_op jit(solution)/shard_map/all_to_all | solution.py:23
  399.2 6.3 %fusion.1 = f32[768,1024]{1,0:T(8,128)S(1)} fusion(bf16[768,2048]{1,0:T(8,128)(2,1)} %bitcast.5, bf16[1024,6144]{1,0:T(8,128)(2,1)} %bitcast.12), kind=kOutput, calls=%fused_computation.4 | convolution fusion | flops 3221225472 | bytes 10485760 | tf_op jit(solution)/shard_map/erd,edf->erf/dot_general | solution.py:137
  405.6 7.0 %multiply_convert_fusion = bf16[768,1024]{1,0:T(8,128)(2,1)S(1)} fusion(f32[768,1024]{1,0:T(8,128)S(1)} %fusion.1, bf16[768,2048]{1,0:T(8,128)(2,1)} %bitcast.5, bf16[1024,6144]{1,0:T(8,128)(2,1)} %bitcast.12), kind=kOutput, calls=%fused_computation.10 | convolution fusion | flops 3225944064 | bytes 12058624 | tf_op jit(solution)/shard_map/erd,edf->erf/dot_general | solution.py:136
  412.6 5.8 %fusion.3 = bf16[768,2048]{1,0:T(8,128)(2,1)S(1)} fusion(bf16[768,1024]{1,0:T(8,128)(2,1)S(1)} %multiply_convert_fusion, bf16[1024,6144]{1,0:T(8,128)(2,1)} %bitcast.12), kind=kOutput, calls=%fused_computation.7 | convolution fusion | flops 3222798336 | bytes 8912896 | tf_op jit(solution)/shard_map/erf,edf->erd/dot_general | solution.py:139
  418.4 1.4 fusion.38
  419.8 0.0 copy-start.6
  419.8 27.0 %all_to_all.24 = bf16[16,1,24,2048]{3,2,1,0:T(8,128)(2,1)S(1)} all-to-all(bf16[16,1,24,2048]{3,2,1,0:T(8,128)(2,1)S(1)} %get-tuple-element.2), channel_id=1, replica_groups=mesh['ep'=16,'tp'=16] {'ep'}, dimensions={0} | all-to-all | bytes 3145728 | tf_op jit(solution)/shard_map/all_to_all | solution.py:61
  446.8 6.0 %all-to-all-start.3 = ((bf16[16,1,24,2048]{3,2,1,0:T(8,128)(2,1)}), bf16[16,1,24,2048]{3,2,1,0:T(8,128)(2,1)S(1)}, u32[]{:S(2)}, u32[]{:S(2)}) async-start(bf16[16,1,24,2048]{3,2,1,0:T(8,128)(2,1)} %get-tuple-element.3), calls=%async_computation.4 | async-start | bytes 3145728 | tf_op jit(solution)/shard_map/all_to_all | solution.py:61
  452.7 0.0 copy-done.6
  452.7 21.8 %all-to-all-done.3 = bf16[16,1,24,2048]{3,2,1,0:T(8,128)(2,1)S(1)} async-done(((bf16[16,1,24,2048]{3,2,1,0:T(8,128)(2,1)}), bf16[16,1,24,2048]{3,2,1,0:T(8,128)(2,1)S(1)}, u32[]{:S(2)}, u32[]{:S(2)}) %all-to-all-start.3) | async-done | bytes 1572896 | tf_op jit(solution)/shard_map/all_to_all | solution.py:61
  474.6 0.2 pad_maximum_fusion
  474.8 1.1 convolution_multiply_fusion.1
  475.9 2.1 fusion.5
  478.0 0.0 reduce-scatter.2.cloned.1.call-done
  (10 shorter events, 0.1 us)
Async XLA Ops:
  7.2 86.3 %copy-start = (bf16[64,2048]{1,0:T(8,128)(2,1)S(1)}, bf16[64,2048]{1,0:T(8,128)(2,1)}, u32[]{:S(2)}) copy-start(bf16[64,2048]{1,0:T(8,128)(2,1)} %param.12) | copy-start | bytes 786436
  16.3 7.3 %copy-start.2 = (bf16[1,2048,64]{1,2,0:T(8,128)(2,1)S(1)}, bf16[1,2048,64]{1,2,0:T(8,128)(2,1)}, u32[]{:S(2)}) copy-start(bf16[1,2048,64]{1,2,0:T(8,128)(2,1)} %param.19) | copy-start | bytes 786436
  16.3 7.3 %copy-start.3 = (bf16[1,2048,64]{1,2,0:T(8,128)(2,1)S(1)}, bf16[1,2048,64]{1,2,0:T(8,128)(2,1)}, u32[]{:S(2)}) copy-start(bf16[1,2048,64]{1,2,0:T(8,128)(2,1)} %param.18) | copy-start | bytes 786436
  16.3 7.3 %copy-start.4 = (bf16[1,2048,64]{1,2,0:T(8,128)(2,1)S(1)}, bf16[1,2048,64]{1,2,0:T(8,128)(2,1)}, u32[]{:S(2)}) copy-start(bf16[1,2048,64]{1,2,0:T(8,128)(2,1)} %param.17) | copy-start | bytes 786436
  16.3 53.6 %all-to-all-start = ((bf16[16,48,2048]{2,1,0:T(8,128)(2,1)}), bf16[16,48,2048]{2,1,0:T(8,128)(2,1)}, u32[]{:S(2)}, u32[]{:S(2)}) async-start(bf16[16,48,2048]{2,1,0:T(8,128)(2,1)} %bitcast.4), calls=%async_computation.1 | async-start | bytes 6291456 | tf_op jit(solution)/shard_map/all_to_all | solution.py:132
  76.0 8.8 %copy-start.1 = (bf16[2048,64]{0,1:T(8,128)(2,1)S(1)}, bf16[2048,64]{0,1:T(8,128)(2,1)}, u32[]{:S(2)}) copy-start(bf16[2048,64]{0,1:T(8,128)(2,1)} %param.10) | copy-start | bytes 786436
  76.0 323.2 %all-to-all-start.1 = ((bf16[16,64,6144]{2,1,0:T(8,128)(2,1)}), bf16[16,64,6144]{2,1,0:T(8,128)(2,1)}, u32[]{:S(2)}, u32[]{:S(2)}) async-start(bf16[16,64,6144]{2,1,0:T(8,128)(2,1)} %stack.2), calls=%async_computation.2 | async-start | bytes 25165824 | tf_op jit(solution)/shard_map/all_to_all | solution.py:23
  84.8 8.7 %copy-start.5 = (f32[64]{0:T(128)S(1)}, f32[64]{0:T(128)}, u32[]{:S(2)}) copy-start(f32[64]{0:T(128)} %param.11) | copy-start | bytes 772
  84.8 393.2 %reduce-scatter.2.cloned.1.call-start = ((), (), s32[]{:S(2)}) async-start(), calls=%async_computation.5 | async-start | bytes 8912896 | tf_op jit(solution)/shard_map/reduce_scatter | solution.py:116
  84.9 7.7 %collective-permute-start = (bf16[15,64]{0,1:T(8,128)(2,1)S(1)}, bf16[15,64]{0,1:T(8,128)(2,1)S(1)}, u32[]{:S(2)}, u32[]{:S(2)}) collective-permute-start(bf16[15,64]{0,1:T(8,128)(2,1)S(1)} %slice.66), channel_id=1, source_target_pairs={{0,16},{16,32},{32,48},{48,64},{64,80},{80,96},{96,112},{112,128},... | collective-permute-start | bytes 5768 | tf_op jit(solution)/shard_map/ppermute | solution.py:16
  419.8 32.9 %copy-start.6 = (f32[256,2]{0,1:T(2,128)S(1)}, f32[256,2]{0,1:T(2,128)}, u32[]{:S(2)}) copy-start(f32[256,2]{0,1:T(2,128)} %param.16) | copy-start | bytes 6148
  446.8 27.8 %all-to-all-start.3 = ((bf16[16,1,24,2048]{3,2,1,0:T(8,128)(2,1)}), bf16[16,1,24,2048]{3,2,1,0:T(8,128)(2,1)S(1)}, u32[]{:S(2)}, u32[]{:S(2)}) async-start(bf16[16,1,24,2048]{3,2,1,0:T(8,128)(2,1)} %get-tuple-element.3), calls=%async_computation.4 | async-start | bytes 3145728 | tf_op jit(solution)/shard_map/all_to_all | solution.py:61
Sparse Core Ops, SparseCore 0:
  100.0 301.9 reduce-scatter.1
